TPU v7x, 512 devices: a whole 4x8x8 slice. The times are simulated.
512 devices in a mesh: rep: 2 (over z_hi), fs: 32 (over z_lo, y), tp: 8 (over x, core).
Axes of the slice: x: 4, y: 8, z: 8 (z_hi: 2, z_lo: 4; z = z_hi * 4 + z_lo), core: 2. Of those that a mesh axis runs over, the one named last changes fastest.
Arguments:
- pre_gate: bfloat16 [49152, 4096], P(('rep', 'fs'), 'tp'), may hold values from -6 to 6
- pre_linear: bfloat16 [49152, 4096], P(('rep', 'fs'), 'tp'), may hold values from -6 to 6
- taps_gate: float32 [3, 4096], P(None, 'tp'), may hold values from -3.5 to 3.5
- taps_linear: float32 [3, 4096], P(None, 'tp'), may hold values from -3.5 to 3.5
- bias_gate: float32 [4096], P('tp'), may hold values from -3 to 3
- bias_linear: float32 [4096], P('tp'), may hold values from -3 to 3
- down_weight: bfloat16 [4096, 2048], P('tp', 'fs'), may hold values from -0.09375 to 0.09375
- out_grad: bfloat16 [49152, 2048], P(('rep', 'fs')), may hold values from -8 to 8
Outputs:
- grad_gate: bfloat16 [49152, 4096], P(('rep', 'fs'), 'tp')
- grad_linear: bfloat16 [49152, 4096], P(('rep', 'fs'), 'tp')
- grad_taps_gate: float32 [3, 4096], P(None, 'tp')
- grad_taps_linear: float32 [3, 4096], P(None, 'tp')
- grad_bias_gate: float32 [4096], P('tp')
- grad_bias_linear: float32 [4096], P('tp')
- grad_down: float32 [4096, 2048], P('tp', 'fs')
- row_norms: float32 [4096], P('tp')
All inputs are finite; a program needn't handle non-finite values.
Results may differ from a plain program's by a relative error of at most 0.0031.
Values may be sent and summed in bfloat16 or wider, within the bound.
A program may use at most 64 MiB of HBM per device.

v0:
```python
import jax
import jax.numpy as jnp
from jax import lax
from jax.sharding import Mesh
from jax.sharding import PartitionSpec as P

FS = ("fs_0", "fs_1")
REP_FS = ("rep", "fs_0", "fs_1")


def joined_along(parts, dim):
    lengths = list(parts.shape[1:])
    lengths[dim] *= parts.shape[0]
    return jnp.moveaxis(parts, 0, dim).reshape(lengths)


def copy_for_each(shard, axis):
    count = lax.axis_size(axis)
    return lax.all_to_all(
        jnp.broadcast_to(shard[None], (count, *shard.shape)), axis, 0, 0, tiled=True
    )


def gather_directly(shard, axis, dim):
    return joined_along(copy_for_each(shard, axis), dim)


def by_axis(shard, axes):
    for axis in axes:
        shard = lax.psum(shard, axis)
    return shard


def sum_in_order(parts, axes, sequence):
    inside = parts.shape[1:]
    parts = parts.reshape(*(lax.axis_size(a) for a in axes), *inside)
    parts = jnp.moveaxis(parts, sequence, range(len(axes))).reshape(-1, *inside)
    for k in sequence:
        parts = lax.psum_scatter(parts, axes[k], scatter_dimension=0, tiled=True)
    return parts[0]


def split_up(shard, dim, count):
    lengths = shard.shape
    parts = shard.reshape(*lengths[:dim], count, lengths[dim] // count, *lengths[dim + 1 :])
    return jnp.moveaxis(parts, dim, 0)


def scatter_axes(shard, axes, sequence, dim):
    count = lax.axis_size(axes)
    return sum_in_order(split_up(shard, dim, count), axes, sequence)


def of_everyone(shard, axis):
    everything = copy_for_each(shard, axis)
    return jnp.sum(everything, axis=0)


def convolve(values, taps, bias):
    length = values.shape[0]
    padded = jnp.pad(values, ((2, 0), (0, 0)))
    return (
        taps[0] * padded[0:length]
        + taps[1] * padded[1 : length + 1]
        + taps[2] * padded[2 : length + 2]
        + bias
    )


def convolve_back(grads, taps):
    length = grads.shape[0]
    padded = jnp.pad(grads, ((0, 2), (0, 0)))
    return (
        taps[0] * padded[2 : length + 2]
        + taps[1] * padded[1 : length + 1]
        + taps[2] * padded[0:length]
    )


def tap_grads(grads, values):
    length = values.shape[0]
    padded = jnp.pad(values, ((2, 0), (0, 0)))
    return jnp.stack([jnp.sum(grads * padded[j : j + length], axis=0) for j in range(3)])


def local(
    pre_gate, pre_linear, taps_gate, taps_linear, bias_gate, bias_linear, down_weight, out_grad
):
    gate_in = pre_gate.astype(jnp.float32)
    linear_in = pre_linear.astype(jnp.float32)
    gate_pre = convolve(gate_in, taps_gate, bias_gate)
    linear_pre = convolve(linear_in, taps_linear, bias_linear)
    sigma = jax.nn.sigmoid(gate_pre)
    silu_val = gate_pre * sigma
    hidden = (silu_val * linear_pre).astype(jnp.bfloat16)
    gathered = gather_directly(down_weight, FS, 1)
    grad_hidden = lax.dot_general(
        out_grad, gathered, (((1,), (1,)), ((), ())), preferred_element_type=jnp.float32
    )
    grad_gate_pre = grad_hidden * linear_pre * sigma * (1.0 + gate_pre * (1.0 - sigma))
    grad_linear_pre = grad_hidden * silu_val
    grad_gate = convolve_back(grad_gate_pre, taps_gate).astype(jnp.bfloat16)
    grad_linear = convolve_back(grad_linear_pre, taps_linear).astype(jnp.bfloat16)
    conv_parts = (
        tap_grads(grad_gate_pre, gate_in),
        tap_grads(grad_linear_pre, linear_in),
        jnp.sum(grad_gate_pre, axis=0),
        jnp.sum(grad_linear_pre, axis=0),
    )
    grad_taps_gate, grad_taps_linear, grad_bias_gate, grad_bias_linear = (
        by_axis(conv_parts[0], REP_FS),
        by_axis(conv_parts[1], REP_FS),
        by_axis(conv_parts[2], REP_FS),
        by_axis(conv_parts[3], REP_FS),
    )
    partial_grad = scatter_axes(
        lax.dot_general(
            out_grad, hidden, (((0,), (0,)), ((), ())), preferred_element_type=jnp.float32
        ),
        FS,
        (1, 0),
        0,
    )
    summed = of_everyone(partial_grad, "rep")
    grad_down = summed.T
    row_norms = by_axis(jnp.sum(grad_down * grad_down, axis=1), FS)
    return (
        grad_gate,
        grad_linear,
        grad_taps_gate,
        grad_taps_linear,
        grad_bias_gate,
        grad_bias_linear,
        grad_down,
        row_norms,
    )


def solution(mesh):
    split = Mesh(
        mesh.devices.reshape(mesh.shape["rep"], 4, 8, mesh.shape["tp"]),
        ("rep", "fs_0", "fs_1", "tp"),
    )
    in_specs = (
        P(REP_FS, "tp"),
        P(REP_FS, "tp"),
        P(None, "tp"),
        P(None, "tp"),
        P("tp"),
        P("tp"),
        P("tp", FS),
        P(REP_FS, None),
    )
    out_specs = (
        P(REP_FS, "tp"),
        P(REP_FS, "tp"),
        P(None, "tp"),
        P(None, "tp"),
        P("tp"),
        P("tp"),
        P("tp", FS),
        P("tp"),
    )
    return jax.shard_map(local, mesh=split, in_specs=in_specs, out_specs=out_specs, check_vma=False)
```

profile of v0, /device:TPU:2, one launch (start us, length us, event | category | flops | bytes accessed | tf_op | source)
XLA Modules:
  0.0 261.0 jit_solution(16937942078931800513)
XLA Ops:
  7.2 0.0 copy-start
  7.2 2.5 broadcast_in_dim.6
  9.7 13.0 %all-to-all-start = ((bf16[32,512,64]{1,2,0:T(8,128)(2,1)}), bf16[32,512,64]{1,2,0:T(8,128)(2,1)}, u32[]{:S(2)}, u32[]{:S(2)}) async-start(bf16[32,512,64]{1,2,0:T(8,128)(2,1)} %broadcast_in_dim.6), calls=%async_computation | async-start | bytes 4194304 | tf_op jit(solution)/shard_map/all_to_all | solution.py:19
  22.8 0.0 reduce-scatter.3.cloned.1.call-start
  22.8 0.0 copy-start.4
  22.8 2.6 convert_element_type.24
  25.4 0.0 copy-done.4
  25.4 1.4 convert_element_type.23
  26.8 0.0 copy-done.6
  26.9 0.0 copy-done.7
  26.9 46.6 %all-to-all-done = bf16[32,512,64]{1,2,0:T(8,128)(2,1)} async-done(((bf16[32,512,64]{1,2,0:T(8,128)(2,1)}), bf16[32,512,64]{1,2,0:T(8,128)(2,1)}, u32[]{:S(2)}, u32[]{:S(2)}) %all-to-all-start) | async-done | bytes 2097184 | tf_op jit(solution)/shard_map/all_to_all | solution.py:19
  73.5 0.0 copy-done.9
  73.5 0.0 copy-start.3
  73.5 0.0 copy-start.8
  73.5 7.1 %fusion.4 = (f32[512]{0:T(512)S(1)}, f32[512]{0:T(512)S(1)}, f32[512]{0:T(512)S(1)}, f32[512]{0:T(512)S(1)}, f32[768,512]{1,0:T(8,128)S(1)}, /*index=5*/f32[768,512]{1,0:T(8,128)S(1)}, f32[768,512]{1,0:T(8,128)S(1)}) fusion(bf16[768,512]{1,0:T(8,128)(2,1)} %param.9, f32[768,512]{1,0:T(8,128)} %convert_element_type.23, f32[512]{0:T(512)S(1)} %copy-done.9, ...), kind=kOutput, calls=%fused_computation.24 | convolution fusion | flops 1618081792 | bytes 13910016 | tf_op jit(solution)/shard_map/dot_general | solution.py:97
  80.7 3.2 %fusion.5 = (f32[512]{0:T(512)S(1)}, f32[512]{0:T(512)S(1)}, f32[512]{0:T(512)S(1)}, f32[512]{0:T(512)S(1)}, f32[768,512]{1,0:T(8,128)}, /*index=5*/f32[768,512]{1,0:T(8,128)S(1)}, bf16[768,512]{1,0:T(8,128)(2,1)}) fusion(bf16[768,512]{1,0:T(8,128)(2,1)S(1)} %copy-done.3, f32[768,512]{1,0:T(8,128)S(1)} %copy-done.1, f32[768,512]{1,0:T(8,128)S(1)} %get-tuple-element.35, ...), kind=kLoop, calls=%fused_computation.25 | loop fusion | flops 11401216 | bytes 12599296 | tf_op jit(solution)/shard_map/reduce_sum | solution.py:107
  83.9 3.9 %convolution_bitcast_fusion = f32[2048,512]{0,1:T(8,128)} fusion(bf16[768,2048]{1,0:T(8,128)(2,1)S(1)} %copy-done, f32[768,512]{1,0:T(8,128)S(1)} %get-tuple-element.37, f32[768,512]{1,0:T(8,128)S(1)} %get-tuple-element.35), kind=kOutput, calls=%fused_computation | convolution fusion | flops 1612972032 | bytes 10485760 | tf_op jit(solution)/shard_map/dot_general | solution.py:117
  87.9 5.3 %copy.19 = f32[2048,512]{1,0:T(8,128)} copy(f32[2048,512]{0,1:T(8,128)} %convolution_bitcast_fusion) | data formatting | bytes 8388608 | tf_op jit(solution)/shard_map/dot_general | solution.py:117
  93.2 4.9 %copy.20 = f32[8,4,64,512]{3,2,1,0:T(8,128)} copy(f32[8,4,64,512]{3,2,0,1:T(8,128)} %bitcast.28) | data formatting | bytes 8388608 | tf_op jit(solution)/shard_map/transpose | solution.py:37
  98.1 0.0 reduce-scatter.3.cloned.1.call-update
  98.1 0.0 reduce-scatter.5.cloned.1.call-start
  98.2 58.8 %reduce-scatter.3.cloned.1.call-done = f32[4,64,512]{2,1,0:T(8,128)} async-done(((f32[32,64,512]{2,1,0:T(8,128)}), f32[4,64,512]{2,1,0:T(8,128)}) %reduce-scatter.3.cloned.1.call-update) | async-done | bytes 524304 | tf_op jit(solution)/shard_map/reduce_scatter | solution.py:39
  157.0 0.0 reduce-scatter.5.cloned.1.call-update
  157.0 17.5 %all-reduce.6 = (f32[3,512]{1,0:T(4,128)S(1)}, f32[3,512]{1,0:T(4,128)S(1)}, f32[512]{0:T(512)}, f32[512]{0:T(512)}) all-reduce(f32[3,512]{1,0:T(4,128)S(1)} %get-tuple-element.46, f32[3,512]{1,0:T(4,128)S(1)} %get-tuple-element.47, f32[512]{0:T(512)S(1)} %get-tuple-element.16, ...), channel_id=1, replica_groups=mesh['rep'=2,'fs_0'=4,'fs_1'=8,'tp'=8] {'rep'}, use_global_device_ids=true, to_apply=%region_3.4 | all-reduce | flops 4096 | bytes 32768 | tf_op jit(solution)/shard_map/psum | solution.py:30
  174.5 14.6 %reduce-scatter.5.cloned.1.call-done = f32[1,64,512]{2,1,0:T(8,128)} async-done(((f32[4,64,512]{2,1,0:T(8,128)}), f32[1,64,512]{2,1,0:T(8,128)}) %reduce-scatter.5.cloned.1.call-update) | async-done | bytes 131088 | tf_op jit(solution)/shard_map/reduce_scatter | solution.py:39
  189.0 1.6 broadcast_in_dim.8
  190.7 4.1 %all-to-all-start.1 = ((f32[2,64,512]{2,1,0:T(8,128)}), f32[2,64,512]{2,1,0:T(8,128)S(1)}, u32[]{:S(2)}, u32[]{:S(2)}) async-start(f32[2,64,512]{2,1,0:T(8,128)} %broadcast_in_dim.8), calls=%async_computation.3 | async-start | bytes 524288 | tf_op jit(solution)/shard_map/all_to_all | solution.py:19
  194.8 4.1 %add_convert_fusion.1 = bf16[768,512]{1,0:T(8,128)(2,1)} fusion(f32[768,512]{1,0:T(8,128)} %get-tuple-element.36, f32[512]{0:T(512)S(1)} %bitcast.40, f32[512]{0:T(512)S(1)} %bitcast.42, f32[512]{0:T(512)S(1)} %bitcast.38), kind=kLoop, calls=%fused_computation.9 | loop fusion | flops 2359296 | bytes 2365440 | tf_op jit(solution)/shard_map/convert_element_type | solution.py:102
  198.9 5.5 %all-to-all-done.1 = f32[2,64,512]{2,1,0:T(8,128)S(1)} async-done(((f32[2,64,512]{2,1,0:T(8,128)}), f32[2,64,512]{2,1,0:T(8,128)S(1)}, u32[]{:S(2)}, u32[]{:S(2)}) %all-to-all-start.1) | async-done | bytes 262176 | tf_op jit(solution)/shard_map/all_to_all | solution.py:19
  204.5 0.0 copy-start.5
  204.5 19.2 %all-reduce.5 = (f32[3,512]{1,0:T(4,128)S(1)}, f32[3,512]{1,0:T(4,128)S(1)}, f32[512]{0:T(512)S(1)}, f32[512]{0:T(512)S(1)}, f32[512]{0:T(512)S(1)}) all-reduce(f32[3,512]{1,0:T(4,128)S(1)} %get-tuple-element.30, f32[3,512]{1,0:T(4,128)S(1)} %get-tuple-element.31, ...), channel_id=1, replica_groups=mesh['rep'=2,'fs_0'=4,'fs_1'=8,'tp'=8] {'fs_0'}, use_global_device_ids=true, to_apply=%region_4.5 | all-reduce | flops 4608 | bytes 36864 | tf_op jit(solution)/shard_map/psum | solution.py:30
  223.7 30.4 %all-reduce.4 = (f32[3,512]{1,0:T(4,128)}, f32[3,512]{1,0:T(4,128)}, f32[512]{0:T(512)}, f32[512]{0:T(512)}, f32[512]{0:T(512)}) all-reduce(f32[3,512]{1,0:T(4,128)S(1)} %get-tuple-element.25, f32[3,512]{1,0:T(4,128)S(1)} %get-tuple-element.26, ...), channel_id=1, replica_groups=mesh['rep'=2,'fs_0'=4,'fs_1'=8,'tp'=8] {'fs_1'}, use_global_device_ids=true, to_apply=%region_5.6 | all-reduce | flops 4608 | bytes 36864 | tf_op jit(solution)/shard_map/psum | solution.py:30
  (16 shorter events, 0.1 us)
Async XLA Ops:
  7.2 66.3 %copy-start = (bf16[768,2048]{1,0:T(8,128)(2,1)S(1)}, bf16[768,2048]{1,0:T(8,128)(2,1)}, u32[]{:S(2)}) copy-start(bf16[768,2048]{1,0:T(8,128)(2,1)} %param.15) | copy-start | bytes 9437188
  9.7 63.8 %all-to-all-start = ((bf16[32,512,64]{1,2,0:T(8,128)(2,1)}), bf16[32,512,64]{1,2,0:T(8,128)(2,1)}, u32[]{:S(2)}, u32[]{:S(2)}) async-start(bf16[32,512,64]{1,2,0:T(8,128)(2,1)} %broadcast_in_dim.6), calls=%async_computation | async-start | bytes 4194304 | tf_op jit(solution)/shard_map/all_to_all | solution.py:19
  22.8 134.2 %reduce-scatter.3.cloned.1.call-start = ((), (), s32[]{:S(2)}) async-start(), calls=%async_computation.4 | async-start | bytes 4718592 | tf_op jit(solution)/shard_map/reduce_scatter | solution.py:39
  22.8 2.6 %copy-start.4 = (bf16[768,512]{1,0:T(8,128)(2,1)S(1)}, bf16[768,512]{1,0:T(8,128)(2,1)}, u32[]{:S(2)}) copy-start(bf16[768,512]{1,0:T(8,128)(2,1)} %param.9) | copy-start | bytes 2359300
  25.4 1.4 copy-start.6
  25.4 1.4 copy-start.7
  25.4 48.1 %copy-start.9 = (f32[512]{0:T(512)S(1)}, f32[512]{0:T(512)}, u32[]{:S(2)}) copy-start(f32[512]{0:T(512)} %param.12) | copy-start | bytes 6148
  73.5 7.1 %copy-start.1 = (f32[768,512]{1,0:T(8,128)S(1)}, f32[768,512]{1,0:T(8,128)}, u32[]{:S(2)}) copy-start(f32[768,512]{1,0:T(8,128)} %convert_element_type.24) | copy-start | bytes 4718596
  73.5 7.1 %copy-start.2 = (f32[768,512]{1,0:T(8,128)S(1)}, f32[768,512]{1,0:T(8,128)}, u32[]{:S(2)}) copy-start(f32[768,512]{1,0:T(8,128)} %convert_element_type.23) | copy-start | bytes 4718596
  73.5 7.2 %copy-start.3 = (bf16[768,512]{1,0:T(8,128)(2,1)S(1)}, bf16[768,512]{1,0:T(8,128)(2,1)}, u32[]{:S(2)}) copy-start(bf16[768,512]{1,0:T(8,128)(2,1)} %param.8) | copy-start | bytes 2359300
  73.5 7.1 %copy-start.8 = (f32[512]{0:T(512)S(1)}, f32[512]{0:T(512)}, u32[]{:S(2)}) copy-start(f32[512]{0:T(512)} %param.13) | copy-start | bytes 6148
  98.1 90.9 %reduce-scatter.5.cloned.1.call-start = ((), (), s32[]{:S(2)}) async-start(), calls=%async_computation.5 | async-start | bytes 655360 | tf_op jit(solution)/shard_map/reduce_scatter | solution.py:39
  190.7 13.8 %all-to-all-start.1 = ((f32[2,64,512]{2,1,0:T(8,128)}), f32[2,64,512]{2,1,0:T(8,128)S(1)}, u32[]{:S(2)}, u32[]{:S(2)}) async-start(f32[2,64,512]{2,1,0:T(8,128)} %broadcast_in_dim.8), calls=%async_computation.3 | async-start | bytes 524288 | tf_op jit(solution)/shard_map/all_to_all | solution.py:19
  204.5 49.7 %copy-start.5 = (f32[64,512]{1,0:T(8,128)}, f32[64,512]{1,0:T(8,128)S(1)}, u32[]{:S(2)}) copy-start(f32[64,512]{1,0:T(8,128)S(1)} %reduce_sum.98) | copy-start | bytes 393220
Sparse Core Ops, SparseCore 0:
  98.2 58.7 reduce-scatter.2
  159.8 29.1 reduce-scatter.4
where the time goes:
time: 261 us
  waiting for transfers between devices  126 us (48%)
  blocking collectives  67.1 us (26%)
  starting transfers between devices  17.3 us (7%)
  local copies, waits for them, and re-layouts  14.4 us (6%)
  between operations  14.2 us (5%)
  other arithmetic  11.4 us (4%)
  matrix products  11 us (4%)
    reduce_scatter x2, waiting for transfers between devices, sum_in_order(): parts = lax.psum_scatter(parts, axes[k], scatter_dimension=0, tiled=True)  73.4 us
    psum x3, blocking collectives, by_axis(): shard = lax.psum(shard, axis)  67.1 us
    all_to_all x2, waiting for transfers between devices, copy_for_each(): lax.all_to_all(jnp.broadcast_to(shard[None], (count, *shard.shape)), axis...  52.1 us
    all_to_all x2, starting transfers between devices, copy_for_each(): lax.all_to_all(jnp.broadcast_to(shard[None], (count, *shard.shape)), axis...  17.2 us
    dot_general x1, matrix products, local(): lax.dot_general(out_grad, gathered, (((1,), (1,)), ((), ())), preferred_e...  7.1 us
    dot_general x1, local copies, waits for them, and re-layouts, local(): lax.dot_general(out_grad, hidden, (((0,), (0,)), ((), ())), preferred_ele...  5.35 us
  transfers between devices with their start and end apart: 4, of which 4 were waited for; matrix products, arithmetic and copies ran while one was open for 3% of the time, Pallas kernels for 0%

commit v1 on v0

--- a/solution.py
+++ b/solution.py
@@ -27,7 +27,8 @@
 
 def by_axis(shard, axes):
     for axis in axes:
-        shard = lax.psum(shard, axis)
+        shards = lax.all_gather(shard, axis, axis=0, tiled=False)
+        shard = shards.sum(axis=0)
     return shard
 
 

time: 261 us -> 395 us (1.51)
  blocking collectives: 67.1 us -> 209 us
  waiting for transfers between devices: 126 us -> 110 us
    all_gather x0 -> x14, blocking collectives: none -> 209 us  [by_axis(): shards = lax.all_gather(shard, axis, axis=0, tiled=False)]
    psum x3 -> x0, blocking collectives: 67.1 us -> none  [by_axis(): shard = lax.psum(shard, axis)]
    reduce_scatter x2, waiting for transfers between devices: 73.4 us -> 58.8 us  [sum_in_order(): parts = lax.psum_scatter(parts, axes[k], scatter_dimension=0, tiled=True)]
  transfers between devices with their start and end apart: 4 -> 4, of which waited for: 4 -> 3; matrix products, arithmetic and copies ran while one was open for 3% -> 3% of each run, Pallas kernels for 0% -> 0%
where the time goes in v1:
time: 395 us; the launch traced here: 394 us
  blocking collectives  209 us (53%)
  waiting for transfers between devices  110 us (28%)
  starting transfers between devices  19.9 us (5%)
  other arithmetic  14.7 us (4%)
  local copies, waits for them, and re-layouts  14.4 us (4%)
  between operations  14.2 us (4%)
  matrix products  11 us (3%)
    all_gather x14, blocking collectives, by_axis(): shards = lax.all_gather(shard, axis, axis=0, tiled=False)  209 us
    reduce_scatter x2, waiting for transfers between devices, sum_in_order(): parts = lax.psum_scatter(parts, axes[k], scatter_dimension=0, tiled=True)  58.8 us
    all_to_all x2, waiting for transfers between devices, copy_for_each(): lax.all_to_all(jnp.broadcast_to(shard[None], (count, *shard.shape)), axis...  51.6 us
    all_to_all x2, starting transfers between devices, copy_for_each(): lax.all_to_all(jnp.broadcast_to(shard[None], (count, *shard.shape)), axis...  19.9 us
  transfers between devices with their start and end apart: 4, of which 3 were waited for; matrix products, arithmetic and copies ran while one was open for 3% of the time, Pallas kernels for 0%

profile of v1, /device:TPU:2, one launch (start us, length us, event | category | flops | bytes accessed | tf_op | source)
XLA Modules:
  0.0 394.1 jit_solution(11294168928086989224)
XLA Ops:
  7.2 2.5 broadcast_in_dim.6
  9.7 13.0 %all-to-all-start = ((bf16[32,512,64]{1,2,0:T(8,128)(2,1)}), bf16[32,512,64]{1,2,0:T(8,128)(2,1)}, u32[]{:S(2)}, u32[]{:S(2)}) async-start(bf16[32,512,64]{1,2,0:T(8,128)(2,1)} %broadcast_in_dim.6), calls=%async_computation | async-start | bytes 4194304 | tf_op jit(solution)/shard_map/all_to_all | solution.py:19
  22.8 2.6 convert_element_type.23
  25.4 1.4 convert_element_type.24
  26.9 46.6 %all-to-all-done = bf16[32,512,64]{1,2,0:T(8,128)(2,1)} async-done(((bf16[32,512,64]{1,2,0:T(8,128)(2,1)}), bf16[32,512,64]{1,2,0:T(8,128)(2,1)}, u32[]{:S(2)}, u32[]{:S(2)}) %all-to-all-start) | async-done | bytes 2097184 | tf_op jit(solution)/shard_map/all_to_all | solution.py:19
  73.5 7.1 %fusion.4 = (f32[512]{0:T(512)S(1)}, f32[512]{0:T(512)S(1)}, f32[512]{0:T(512)S(1)}, f32[512]{0:T(512)S(1)}, f32[768,512]{1,0:T(8,128)S(1)}, /*index=5*/f32[768,512]{1,0:T(8,128)S(1)}, f32[768,512]{1,0:T(8,128)S(1)}) fusion(bf16[768,512]{1,0:T(8,128)(2,1)} %param.9, f32[768,512]{1,0:T(8,128)} %convert_element_type.23, f32[512]{0:T(512)S(1)} %copy-done.9, ...), kind=kOutput, calls=%fused_computation.24 | convolution fusion | flops 1618081792 | bytes 13910016 | tf_op jit(solution)/shard_map/dot_general | solution.py:98
  80.7 3.2 fusion.5
  83.9 3.9 %convolution_bitcast_fusion = f32[2048,512]{0,1:T(8,128)} fusion(bf16[768,2048]{1,0:T(8,128)(2,1)S(1)} %copy-done, f32[768,512]{1,0:T(8,128)S(1)} %get-tuple-element.23, f32[768,512]{1,0:T(8,128)S(1)} %get-tuple-element.21), kind=kOutput, calls=%fused_computation | convolution fusion | flops 1612972032 | bytes 10485760 | tf_op jit(solution)/shard_map/dot_general | solution.py:118
  87.9 5.3 %copy.21 = f32[2048,512]{1,0:T(8,128)} copy(f32[2048,512]{0,1:T(8,128)} %convolution_bitcast_fusion) | data formatting | bytes 8388608 | tf_op jit(solution)/shard_map/dot_general | solution.py:118
  93.2 4.9 %copy.22 = f32[8,4,64,512]{3,2,1,0:T(8,128)} copy(f32[8,4,64,512]{3,2,0,1:T(8,128)} %bitcast.44) | data formatting | bytes 8388608 | tf_op jit(solution)/shard_map/transpose | solution.py:38
  98.2 58.8 %reduce-scatter.3.cloned.1.call-done = f32[4,64,512]{2,1,0:T(8,128)} async-done(((f32[32,64,512]{2,1,0:T(8,128)}), f32[4,64,512]{2,1,0:T(8,128)}) %reduce-scatter.3.cloned.1.call-update) | async-done | bytes 524304 | tf_op jit(solution)/shard_map/reduce_scatter | solution.py:40
  157.0 8.4 %all-gather.14 = f32[2,3,512]{2,1,0:T(4,128)S(1)} all-gather(f32[1,3,512]{2,1,0:T(4,128)S(1)} %maximum_bitcast_fusion), channel_id=2, replica_groups=mesh['rep'=2,'fs_0'=4,'fs_1'=8,'tp'=8] {'rep'}, dimensions={0}, use_global_device_ids=true | all-gather | bytes 18432 | tf_op jit(solution)/shard_map/all_gather | solution.py:30
  165.4 13.4 %all-gather.15 = f32[4,3,512]{2,1,0:T(4,128)S(1)} all-gather(f32[1,3,512]{2,1,0:T(4,128)S(1)} %bitcast.47), channel_id=3, replica_groups=mesh['rep'=2,'fs_0'=4,'fs_1'=8,'tp'=8] {'fs_0'}, dimensions={0}, use_global_device_ids=true | all-gather | bytes 30720 | tf_op jit(solution)/shard_map/all_gather | solution.py:30
  178.9 24.6 %all-gather.16 = f32[8,3,512]{2,1,0:T(4,128)S(1)} all-gather(f32[1,3,512]{2,1,0:T(4,128)S(1)} %bitcast.49), channel_id=4, replica_groups=mesh['rep'=2,'fs_0'=4,'fs_1'=8,'tp'=8] {'fs_1'}, dimensions={0}, use_global_device_ids=true | all-gather | bytes 55296 | tf_op jit(solution)/shard_map/all_gather | solution.py:30
  203.5 0.6 reduce_sum.221
  204.1 8.3 %all-gather.20 = f32[2,1,512]{2,1,0:T(1,128)S(1)} all-gather(f32[1,1,512]{2,1,0:T(1,128)S(1)} %bitcast.51), channel_id=8, replica_groups=mesh['rep'=2,'fs_0'=4,'fs_1'=8,'tp'=8] {'rep'}, dimensions={0}, use_global_device_ids=true | all-gather | bytes 6144 | tf_op jit(solution)/shard_map/all_gather | solution.py:30
  212.4 11.9 %all-gather.21 = f32[4,1,512]{2,1,0:T(1,128)S(1)} all-gather(f32[1,1,512]{2,1,0:T(1,128)S(1)} %bitcast.59), channel_id=9, replica_groups=mesh['rep'=2,'fs_0'=4,'fs_1'=8,'tp'=8] {'fs_0'}, dimensions={0}, use_global_device_ids=true | all-gather | bytes 10240 | tf_op jit(solution)/shard_map/all_gather | solution.py:30
  224.4 21.5 %all-gather.22 = f32[8,1,512]{2,1,0:T(1,128)S(1)} all-gather(f32[1,1,512]{2,1,0:T(1,128)S(1)} %bitcast.61), channel_id=10, replica_groups=mesh['rep'=2,'fs_0'=4,'fs_1'=8,'tp'=8] {'fs_1'}, dimensions={0}, use_global_device_ids=true | all-gather | bytes 18432 | tf_op jit(solution)/shard_map/all_gather | solution.py:30
  246.5 8.3 %all-gather.17 = f32[2,3,512]{2,1,0:T(4,128)S(1)} all-gather(f32[1,3,512]{2,1,0:T(4,128)S(1)} %maximum_bitcast_fusion.1), channel_id=5, replica_groups=mesh['rep'=2,'fs_0'=4,'fs_1'=8,'tp'=8] {'rep'}, dimensions={0}, use_global_device_ids=true | all-gather | bytes 18432 | tf_op jit(solution)/shard_map/all_gather | solution.py:30
  254.8 13.1 %all-gather.18 = f32[4,3,512]{2,1,0:T(4,128)S(1)} all-gather(f32[1,3,512]{2,1,0:T(4,128)S(1)} %bitcast.48), channel_id=6, replica_groups=mesh['rep'=2,'fs_0'=4,'fs_1'=8,'tp'=8] {'fs_0'}, dimensions={0}, use_global_device_ids=true | all-gather | bytes 30720 | tf_op jit(solution)/shard_map/all_gather | solution.py:30
  268.0 24.6 %all-gather.19 = f32[8,3,512]{2,1,0:T(4,128)S(1)} all-gather(f32[1,3,512]{2,1,0:T(4,128)S(1)} %bitcast.50), channel_id=7, replica_groups=mesh['rep'=2,'fs_0'=4,'fs_1'=8,'tp'=8] {'fs_1'}, dimensions={0}, use_global_device_ids=true | all-gather | bytes 55296 | tf_op jit(solution)/shard_map/all_gather | solution.py:30
  292.6 0.6 reduce_sum.227
  293.2 8.3 %all-gather.23 = f32[2,1,512]{2,1,0:T(1,128)S(1)} all-gather(f32[1,1,512]{2,1,0:T(1,128)S(1)} %bitcast.70), channel_id=11, replica_groups=mesh['rep'=2,'fs_0'=4,'fs_1'=8,'tp'=8] {'rep'}, dimensions={0}, use_global_device_ids=true | all-gather | bytes 6144 | tf_op jit(solution)/shard_map/all_gather | solution.py:30
  301.5 12.2 %all-gather.24 = f32[4,1,512]{2,1,0:T(1,128)S(1)} all-gather(f32[1,1,512]{2,1,0:T(1,128)S(1)} %bitcast.60), channel_id=12, replica_groups=mesh['rep'=2,'fs_0'=4,'fs_1'=8,'tp'=8] {'fs_0'}, dimensions={0}, use_global_device_ids=true | all-gather | bytes 10240 | tf_op jit(solution)/shard_map/all_gather | solution.py:30
  313.7 21.1 %all-gather.25 = f32[8,1,512]{2,1,0:T(1,128)S(1)} all-gather(f32[1,1,512]{2,1,0:T(1,128)S(1)} %bitcast.62), channel_id=13, replica_groups=mesh['rep'=2,'fs_0'=4,'fs_1'=8,'tp'=8] {'fs_1'}, dimensions={0}, use_global_device_ids=true | all-gather | bytes 18432 | tf_op jit(solution)/shard_map/all_gather | solution.py:30
  335.5 1.6 broadcast_in_dim.8
  337.1 6.8 %all-to-all-start.1 = ((f32[2,64,512]{2,1,0:T(8,128)}), f32[2,64,512]{2,1,0:T(8,128)S(1)}, u32[]{:S(2)}, u32[]{:S(2)}) async-start(f32[2,64,512]{2,1,0:T(8,128)} %broadcast_in_dim.8), calls=%async_computation.3 | async-start | bytes 524288 | tf_op jit(solution)/shard_map/all_to_all | solution.py:19
  343.9 4.1 %add_convert_fusion.1 = bf16[768,512]{1,0:T(8,128)(2,1)} fusion(f32[768,512]{1,0:T(8,128)} %get-tuple-element.22, f32[512]{0:T(512)S(1)} %bitcast.67, f32[512]{0:T(512)S(1)} %bitcast.69, f32[512]{0:T(512)S(1)} %bitcast.65), kind=kLoop, calls=%fused_computation.9 | loop fusion | flops 2359296 | bytes 2365440 | tf_op jit(solution)/shard_map/convert_element_type | solution.py:103
  348.0 5.0 %all-to-all-done.1 = f32[2,64,512]{2,1,0:T(8,128)S(1)} async-done(((f32[2,64,512]{2,1,0:T(8,128)}), f32[2,64,512]{2,1,0:T(8,128)S(1)}, u32[]{:S(2)}, u32[]{:S(2)}) %all-to-all-start.1) | async-done | bytes 262176 | tf_op jit(solution)/shard_map/all_to_all | solution.py:19
  353.1 11.9 %all-gather.26 = f32[4,1,512]{2,1,0:T(1,128)S(1)} all-gather(f32[1,1,512]{2,1,0:T(1,128)S(1)} %bitcast.55), channel_id=14, replica_groups=mesh['rep'=2,'fs_0'=4,'fs_1'=8,'tp'=8] {'fs_0'}, dimensions={0}, use_global_device_ids=true | all-gather | bytes 10240 | tf_op jit(solution)/shard_map/all_gather | solution.py:30
  365.0 21.7 %all-gather.27 = f32[8,1,512]{2,1,0:T(1,128)S(1)} all-gather(f32[1,1,512]{2,1,0:T(1,128)S(1)} %bitcast.63), channel_id=15, replica_groups=mesh['rep'=2,'fs_0'=4,'fs_1'=8,'tp'=8] {'fs_1'}, dimensions={0}, use_global_device_ids=true | all-gather | bytes 18432 | tf_op jit(solution)/shard_map/all_gather | solution.py:30
  386.7 0.6 reduce_sum.239
  (42 shorter events, 1.6 us)
Async XLA Ops:
  7.2 66.3 %copy-start = (bf16[768,2048]{1,0:T(8,128)(2,1)S(1)}, bf16[768,2048]{1,0:T(8,128)(2,1)}, u32[]{:S(2)}) copy-start(bf16[768,2048]{1,0:T(8,128)(2,1)} %param.15) | copy-start | bytes 9437188
  9.7 63.8 %all-to-all-start = ((bf16[32,512,64]{1,2,0:T(8,128)(2,1)}), bf16[32,512,64]{1,2,0:T(8,128)(2,1)}, u32[]{:S(2)}, u32[]{:S(2)}) async-start(bf16[32,512,64]{1,2,0:T(8,128)(2,1)} %broadcast_in_dim.6), calls=%async_computation | async-start | bytes 4194304 | tf_op jit(solution)/shard_map/all_to_all | solution.py:19
  22.8 134.2 %reduce-scatter.3.cloned.1.call-start = ((), (), s32[]{:S(2)}) async-start(), calls=%async_computation.4 | async-start | bytes 4718592 | tf_op jit(solution)/shard_map/reduce_scatter | solution.py:40
  22.8 2.6 copy-start.3
  25.4 1.4 copy-start.6
  25.4 1.4 copy-start.7
  25.4 48.1 %copy-start.9 = (f32[512]{0:T(512)S(1)}, f32[512]{0:T(512)}, u32[]{:S(2)}) copy-start(f32[512]{0:T(512)} %param.12) | copy-start | bytes 6148
  73.5 7.1 %copy-start.1 = (f32[768,512]{1,0:T(8,128)S(1)}, f32[768,512]{1,0:T(8,128)}, u32[]{:S(2)}) copy-start(f32[768,512]{1,0:T(8,128)} %convert_element_type.23) | copy-start | bytes 4718596
  73.5 7.1 %copy-start.2 = (f32[768,512]{1,0:T(8,128)S(1)}, f32[768,512]{1,0:T(8,128)}, u32[]{:S(2)}) copy-start(f32[768,512]{1,0:T(8,128)} %convert_element_type.24) | copy-start | bytes 4718596
  73.5 7.1 %copy-start.4 = (bf16[768,512]{1,0:T(8,128)(2,1)S(1)}, bf16[768,512]{1,0:T(8,128)(2,1)}, u32[]{:S(2)}) copy-start(bf16[768,512]{1,0:T(8,128)(2,1)} %param.8) | copy-start | bytes 2359300
  73.5 7.1 %copy-start.8 = (f32[512]{0:T(512)S(1)}, f32[512]{0:T(512)}, u32[]{:S(2)}) copy-start(f32[512]{0:T(512)} %param.13) | copy-start | bytes 6148
  98.1 237.4 %reduce-scatter.5.cloned.1.call-start = ((), (), s32[]{:S(2)}) async-start(), calls=%async_computation.5 | async-start | bytes 655360 | tf_op jit(solution)/shard_map/reduce_scatter | solution.py:40
  337.1 15.9 %all-to-all-start.1 = ((f32[2,64,512]{2,1,0:T(8,128)}), f32[2,64,512]{2,1,0:T(8,128)S(1)}, u32[]{:S(2)}, u32[]{:S(2)}) async-start(f32[2,64,512]{2,1,0:T(8,128)} %broadcast_in_dim.8), calls=%async_computation.3 | async-start | bytes 524288 | tf_op jit(solution)/shard_map/all_to_all | solution.py:19
  353.0 34.3 %copy-start.5 = (f32[64,512]{1,0:T(8,128)}, f32[64,512]{1,0:T(8,128)S(1)}, u32[]{:S(2)}) copy-start(f32[64,512]{1,0:T(8,128)S(1)} %reduce_sum.236) | copy-start | bytes 393220
Sparse Core Ops, SparseCore 0:
  98.2 58.7 reduce-scatter.2
  159.8 29.2 reduce-scatter.4
